TPU v7x, 32 devices: a whole 2x2x4 slice. The times are simulated.
32 devices in a mesh: ep: 8 (over z, core), tp: 4 (over y, x).
Axes of the slice: x: 2, y: 2, z: 4, core: 2. Of those that a mesh axis runs over, the one named last changes fastest.
Arguments:
- queries: bfloat16 [2048, 2048], P('ep', 'tp'), may hold values from -6 to 6
- keys: bfloat16 [2048, 2048], P('ep', 'tp'), may hold values from -6 to 6
- values: bfloat16 [2048, 2048], P('ep', 'tp'), may hold values from -6 to 6
- gates: bfloat16 [2048, 2048], P('ep', 'tp'), may hold values from -6 to 6
- log_decay: float32 [2048, 16], P('ep', 'tp'), may hold values from -2 to 0
- out_weight: bfloat16 [2048, 2048], P(None, 'tp'), may hold values from -0.125 to 0.125
- moe_rows: bfloat16 [2048, 2048], P('ep'), may hold values from -140 to 140
- moe_gain: bfloat16 [2048], replicated, may hold values from 0.099609375 to 1.8984375
- routes: int32 [2048, 2], P('ep'), may hold values from 0 to 7, as said below
- route_weights: float32 [2048, 2], P('ep'), may hold values from 0.1 to 1
- gate_proj: bfloat16 [8, 2048, 4096], P('ep', None, 'tp'), may hold values from -0.125 to 0.125
- up_proj: bfloat16 [8, 2048, 4096], P('ep', None, 'tp'), may hold values from -0.125 to 0.125
- down_proj: bfloat16 [8, 4096, 2048], P('ep', None, 'tp'), may hold values from -0.09375 to 0.09375
Outputs:
- mixer_out: bfloat16 [2048, 2048], P('ep', 'tp')
- moe_out: bfloat16 [2048, 2048], P('ep', 'tp')
Inputs may be any that keep to these rules, and one draw needn't show every extreme that they name: `routes`: each row names two different experts of one group of 8 consecutive experts; in each aligned block of 256 rows every expert is named by exactly 64 rows.
All inputs are finite; a program needn't handle non-finite values.
Results may differ from a plain program's by a relative error of at most 0.011.
Values may be sent and summed in bfloat16 or wider, within the bound.
A program may use at most 64 MiB of HBM per device.

v0:
```python
import jax
import jax.numpy as jnp
from jax import lax
from jax.sharding import PartitionSpec as P

BLOCK = 128


def carried_in(value, axis, join, neutral):
    count, mine = (lax.axis_size(axis), lax.axis_index(axis))
    pieces = jax.tree.map(lambda part: lax.all_gather(part, axis), value)
    total = jax.tree.map(
        lambda part, zero: jnp.full_like(part, 0) + jnp.asarray(zero, part.dtype), value, neutral
    )

    def turn(position, total):
        longer = join(total, jax.tree.map(lambda part: part[position], pieces))
        return jax.tree.map(lambda new, old: jnp.where(position < mine, new, old), longer, total)

    return lax.fori_loop(0, count - 1, turn, total)


def rotate(source, positions, heads_here, factor):
    row_count, feat_width = source.shape
    head_dim = feat_width // heads_here
    half_dim = head_dim // 2
    values_f = source.astype(jnp.float32).reshape(row_count, heads_here, head_dim)
    inverse = 10000.0 ** (-jnp.arange(half_dim, dtype=jnp.float32) / half_dim)
    angles = positions[:, None] * inverse[None, :]
    cosine = jnp.cos(angles)[:, None, :]
    sine_part = jnp.sin(angles)[:, None, :]
    first_half = values_f[..., :half_dim]
    second_half = values_f[..., half_dim:]
    turned = jnp.concatenate(
        [
            first_half * cosine - second_half * sine_part,
            first_half * sine_part + second_half * cosine,
        ],
        axis=-1,
    )
    return (turned * factor).astype(jnp.bfloat16).reshape(row_count, feat_width)


def chain_states(earlier, later):
    return (earlier[0] * later[0], later[0][:, None, None] * earlier[1] + later[1])


def retention_half(queries, keys, values, gates, log_decay, out_weight):
    row_count, feat_width = queries.shape
    heads_here = log_decay.shape[1]
    head_dim = feat_width // heads_here
    block_count = row_count // BLOCK
    positions = (lax.axis_index("ep") * row_count + jnp.arange(row_count, dtype=jnp.int32)).astype(
        jnp.float32
    )
    rot_q = rotate(queries, positions, heads_here, 1.0)
    rot_k = rotate(keys, positions, heads_here, head_dim ** (-0.5))
    block_shape = (block_count, BLOCK, heads_here, head_dim)
    q_blocks = rot_q.reshape(block_shape)
    k_blocks = rot_k.reshape(block_shape)
    v_blocks = values.reshape(block_shape)
    cumulative = jnp.cumsum(log_decay.reshape(block_count, BLOCK, heads_here), axis=1)
    across = jnp.swapaxes(cumulative, 1, 2)
    spread = across[..., :, None] - across[..., None, :]
    causal = jnp.arange(BLOCK)[:, None] >= jnp.arange(BLOCK)[None, :]
    weights = jnp.where(causal, jnp.exp(jnp.where(causal, spread, 0.0)), 0.0)
    scores = jnp.einsum("nihd,njhd->nhij", q_blocks, k_blocks, preferred_element_type=jnp.float32)
    rounded = (scores * weights).astype(jnp.bfloat16)
    inside = jnp.einsum("nhij,njhd->nihd", rounded, v_blocks, preferred_element_type=jnp.float32)
    ending = cumulative[:, -1, :]
    k_scaled = k_blocks.astype(jnp.float32) * jnp.exp(ending[:, None, :] - cumulative)[..., None]
    updates = jnp.einsum(
        "njhd,njhe->nhde", k_scaled, v_blocks.astype(jnp.float32), precision=lax.Precision.HIGHEST
    )

    def advance(carry_state, member):
        return (jnp.exp(member[0])[:, None, None] * carry_state + member[1], carry_state)

    zero_state = jnp.zeros((heads_here, head_dim, head_dim), jnp.float32)
    local_end, before = lax.scan(advance, zero_state, (ending, updates))
    device_decay = jnp.exp(jnp.sum(ending, axis=0))
    incoming = carried_in(
        (device_decay, local_end), "ep", chain_states, (jnp.ones_like(device_decay), zero_state)
    )
    leading = jnp.cumsum(ending, axis=0) - ending
    entering = before + jnp.exp(leading)[:, :, None, None] * incoming[1][None]
    carried = (
        jnp.einsum(
            "nihd,nhde->nihe",
            q_blocks.astype(jnp.float32),
            entering,
            precision=lax.Precision.HIGHEST,
        )
        * jnp.exp(cumulative)[..., None]
    )
    retained = (inside + carried).reshape(row_count, heads_here, head_dim)
    gate_f = gates.astype(jnp.float32).reshape(row_count, heads_here, head_dim)
    scaled = retained * lax.rsqrt(jnp.mean(retained * retained, axis=-1, keepdims=True) + 1e-05)
    head_out = (scaled * jax.nn.silu(gate_f)).astype(jnp.bfloat16).reshape(row_count, feat_width)
    projected = jnp.dot(
        lax.all_gather(head_out, "tp", axis=1, tiled=True),
        out_weight,
        preferred_element_type=jnp.float32,
    )
    return projected.astype(jnp.bfloat16)


def expert_half(moe_rows, moe_gain, routes, route_weights, gate_proj, up_proj, down_proj):
    row_count, feat_width = moe_rows.shape
    experts = lax.axis_size("ep")
    capacity = 2 * row_count // experts
    as_float = moe_rows.astype(jnp.float32)
    normed = (
        as_float
        * lax.rsqrt(jnp.mean(as_float * as_float, axis=-1, keepdims=True) + 1e-06)
        * moe_gain.astype(jnp.float32)
    ).astype(jnp.bfloat16)
    flat_ids = routes.reshape(-1)
    onehot = (flat_ids[:, None] == jnp.arange(experts, dtype=jnp.int32)[None, :]).astype(jnp.int32)
    slot_rank = jnp.sum((jnp.cumsum(onehot, axis=0) - onehot) * onehot, axis=1)
    target = flat_ids * capacity + slot_rank
    source_row = (
        jnp.zeros((experts * capacity,), jnp.int32)
        .at[target]
        .set(jnp.arange(2 * row_count, dtype=jnp.int32) // 2)
    )
    outgoing = normed[source_row].reshape(experts, capacity, feat_width)
    w_gate = gate_proj[0]
    w_up = up_proj[0]
    w_down = down_proj[0]
    arrived_rows = lax.all_to_all(outgoing, "ep", split_axis=0, concat_axis=0, tiled=True)
    gate_part = jnp.einsum("scd,df->scf", arrived_rows, w_gate, preferred_element_type=jnp.float32)
    up_part = jnp.einsum("scd,df->scf", arrived_rows, w_up, preferred_element_type=jnp.float32)
    hidden = (jax.nn.silu(gate_part) * up_part).astype(jnp.bfloat16)
    expert_out = jnp.einsum(
        "scf,fd->scd",
        lax.all_gather(hidden, "tp", axis=2, tiled=True),
        w_down,
        preferred_element_type=jnp.float32,
    ).astype(jnp.bfloat16)
    returned = lax.all_to_all(expert_out, "ep", split_axis=0, concat_axis=0, tiled=True)
    picked = returned.reshape(experts * capacity, -1)[target].reshape(row_count, 2, -1)
    return jnp.sum(picked.astype(jnp.float32) * route_weights[:, :, None], axis=1).astype(
        jnp.bfloat16
    )


def on_device(
    queries,
    keys,
    values,
    gates,
    log_decay,
    out_weight,
    moe_rows,
    moe_gain,
    routes,
    route_weights,
    gate_proj,
    up_proj,
    down_proj,
):
    mixer_out = retention_half(queries, keys, values, gates, log_decay, out_weight)
    moe_out = expert_half(moe_rows, moe_gain, routes, route_weights, gate_proj, up_proj, down_proj)
    return (mixer_out, moe_out)


def solution(mesh):
    placed = (
        P("ep", "tp"),
        P("ep", "tp"),
        P("ep", "tp"),
        P("ep", "tp"),
        P("ep", "tp"),
        P(None, "tp"),
        P("ep", None),
        P(),
        P("ep", None),
        P("ep", None),
        P("ep", None, "tp"),
        P("ep", None, "tp"),
        P("ep", None, "tp"),
    )
    return jax.shard_map(
        on_device,
        mesh=mesh,
        in_specs=placed,
        out_specs=(P("ep", "tp"), P("ep", "tp")),
        check_vma=False,
    )
```

profile of v0, /device:TPU:0, one launch (start us, length us, event | category | flops | bytes accessed | tf_op | source)
XLA Modules:
  0.0 199.5 jit_solution(13536535929649242897)
XLA Ops:
  10.9 2.4 %scatter_custom_fusion = s32[512]{0:T(512)S(1)} fusion(s32[512]{0:T(512)S(1)} %bitcast.110, s32[512]{0:T(512)S(1)} %add_select_fusion, s32[]{:T(128)} %copy.125), kind=kCustom, calls=%fused_computation.90 | custom fusion | bytes 2052 | tf_op jit(solution)/shard_map/scatter | solution.py:125
  15.6 1.5 fusion.11
  17.2 3.3 %gather_fusion = bf16[512,2048]{1,0:T(8,128)(2,1)} fusion(bf16[256,2048]{1,0:T(8,128)(2,1)S(1)} %fusion.11, s32[1024]{0:T(1024)S(1)} %pad_clamp_fusion.1), kind=kCustom, calls=%fused_computation | custom fusion | bytes 4196352 | tf_op jit(solution)/shard_map/gather | solution.py:127
  20.5 6.5 %all-to-all-start = ((bf16[8,64,2048]{2,1,0:T(8,128)(2,1)}), bf16[8,64,2048]{2,1,0:T(8,128)(2,1)}, u32[]{:S(2)}, u32[]{:S(2)}) async-start(bf16[8,64,2048]{2,1,0:T(8,128)(2,1)} %bitcast.100), calls=%async_computation | async-start | bytes 4194304 | tf_op jit(solution)/shard_map/all_to_all | solution.py:131
  30.9 1.8 concatenate.21
  37.5 1.7 reshape.218
  40.1 1.7 fusion.27
  41.8 1.7 while.29
  44.3 48.7 %all-to-all-done = bf16[8,64,2048]{2,1,0:T(8,128)(2,1)} async-done(((bf16[8,64,2048]{2,1,0:T(8,128)(2,1)}), bf16[8,64,2048]{2,1,0:T(8,128)(2,1)}, u32[]{:S(2)}, u32[]{:S(2)}) %all-to-all-start) | async-done | bytes 2097184 | tf_op jit(solution)/shard_map/all_to_all | solution.py:131
  92.9 5.3 %fusion.7 = f32[8,64,1024]{2,1,0:T(8,128)S(1)} fusion(bf16[8,64,2048]{2,1,0:T(8,128)(2,1)} %all-to-all-done, bf16[1,2048,1024]{2,1,0:T(8,128)(2,1)} %param.27), kind=kOutput, calls=%fused_computation.15 | convolution fusion | flops 2147483648 | bytes 8388608 | tf_op jit(solution)/shard_map/scd,df->scf/dot_general | solution.py:132
  98.3 5.2 %multiply_convert_fusion = bf16[8,64,1024]{2,1,0:T(8,128)(2,1)} fusion(f32[8,64,1024]{2,1,0:T(8,128)S(1)} %fusion.7, bf16[8,64,2048]{2,1,0:T(8,128)(2,1)} %all-to-all-done, bf16[1,2048,1024]{2,1,0:T(8,128)(2,1)S(1)} %copy-done.11), kind=kOutput, calls=%fused_computation.22 | convolution fusion | flops 2150629376 | bytes 9437184 | tf_op jit(solution)/shard_map/scd,df->scf/dot_general | solution.py:133
  105.0 14.7 %all-reduce = f32[32]{0:T(128)S(1)} all-reduce(f32[32]{0:T(128)S(1)} %exponential_dynamic-update-slice_fusion), channel_id=2, replica_groups=mesh['ep'=8,'tp'=4] {'ep'}, use_global_device_ids=true, to_apply=%add | all-reduce | flops 32 | bytes 256
  121.2 12.4 %while.30 = (s32[]{:T(128)}, f32[4,128,128]{2,1,0:T(8,128)S(1)}, s32[]{:T(128)}, f32[8,4]{1,0:T(8,128)}, f32[8,4,128,128]{3,2,1,0:T(8,128)}) while((s32[]{:T(128)}, f32[4,128,128]{2,1,0:T(8,128)S(1)}, s32[]{:T(128)}, f32[8,4]{1,0:T(8,128)}, f32[8,4,128,128]{3,2,1,0:T(8,128)}) %tuple.79), condition=%wide.region_6.7_spmd.clone.clone, body=%wide.region_5.6_spmd.clone.sunk.clone | while | flops 262148 | bytes 786569 | solution.py:20
  133.6 2.5 %fusion.18 = f32[2,128,4,128]{1,3,2,0:T(8,128)} fusion(f32[2,4,128,128]{3,2,1,0:T(8,128)} %get-tuple-element.124, f32[2,128,4]{1,2,0:T(4,128)S(1)} %copy.82, f32[4,128,128]{2,1,0:T(8,128)S(1)} %get-tuple-element.126, f32[2,4]{1,0:T(2,128)S(1)} %subtract_exponential_fusion.1, bf16[2,128,4,64]{3,1,2,0:T(8,128)(2,1)S(1)} %copy.69, ...), kind=kOutput, calls=%fused_computation.28 | convolution fusion | flops 202244096 | bytes 1576992 | tf_op jit(solution)/shard_map/nihd,nhde->nihe/dot_general | solution.py:88
  136.1 2.4 %multiply_reduce_fusion.1 = (f32[2,128,4]{1,2,0:T(4,128)S(1)}, f32[2,128,4,128]{1,3,2,0:T(8,128)}) fusion(f32[2,128,4,128]{1,3,2,0:T(8,128)} %fusion.18, bf16[2,128,4,128]{3,2,1,0:T(4,128)(2,1)S(1)} %copy-done.4, bf16[2,128,4,128]{3,1,2,0:T(8,128)(2,1)S(1)} %copy-done.3, f32[2,4,128]{2,1,0:T(4,128)S(1)} %copy.75, ...), kind=kOutput, calls=%fused_computation.41 | convolution fusion | flops 68680704 | bytes 1859584 | tf_op jit(solution)/shard_map/nhij,njhd->nihd/dot_general | solution.py:69
  140.3 1.8 fusion.34
  142.2 13.0 %all-gather.8.cloned.1.call-done = bf16[8,64,4096]{2,1,0:T(8,128)(2,1)} async-done(((bf16[8,64,1024]{2,1,0:T(8,128)(2,1)}), bf16[8,64,4096]{2,1,0:T(8,128)(2,1)}) %all-gather.8.cloned.1.call-update) | async-done | bytes 4194320 | tf_op jit(solution)/shard_map/all_gather | solution.py:137
  155.2 6.6 %fusion.14 = bf16[8,64,512]{2,1,0:T(8,128)(2,1)} fusion(bf16[8,64,4096]{2,1,0:T(8,128)(2,1)} %all-gather.8.cloned.1.call-done, bf16[1,4096,512]{2,1,0:T(8,128)(2,1)} %param.29), kind=kOutput, calls=%fused_computation.23 | convolution fusion | flops 2147745792 | bytes 8912896 | tf_op jit(solution)/shard_map/scf,fd->scd/dot_general | solution.py:135
  161.8 4.6 %all-to-all-start.1 = ((bf16[8,64,512]{2,1,0:T(8,128)(2,1)}), bf16[8,64,512]{2,1,0:T(8,128)(2,1)S(1)}, u32[]{:S(2)}, u32[]{:S(2)}) async-start(bf16[8,64,512]{2,1,0:T(8,128)(2,1)} %fusion.14), calls=%async_computation.1 | async-start | bytes 1048576 | tf_op jit(solution)/shard_map/all_to_all | solution.py:141
  166.5 17.4 %all-gather.6.cloned.1.call-done = bf16[256,2048]{1,0:T(8,128)(2,1)} async-done(((bf16[256,512]{1,0:T(8,128)(2,1)}), bf16[256,2048]{1,0:T(8,128)(2,1)}) %all-gather.6.cloned.1.call-update) | async-done | bytes 1048592 | tf_op jit(solution)/shard_map/all_gather | solution.py:101
  184.0 2.6 %convolution_convert_fusion = bf16[256,512]{1,0:T(8,128)(2,1)} fusion(bf16[256,2048]{1,0:T(8,128)(2,1)} %all-gather.6.cloned.1.call-done, bf16[2048,512]{1,0:T(8,128)(2,1)S(1)} %copy-done), kind=kOutput, calls=%fused_computation.29 | convolution fusion | flops 537001984 | bytes 3407872 | tf_op jit(solution)/shard_map/dot_general | solution.py:100
  186.6 2.6 %gather_fusion.1 = bf16[512,512]{1,0:T(8,128)(2,1)} fusion(bf16[512,512]{1,0:T(8,128)(2,1)S(1)} %bitcast.99, s32[1024]{0:T(1024)S(1)} %pad_clamp_fusion), kind=kCustom, calls=%fused_computation.1 | custom fusion | bytes 1050624 | tf_op jit(solution)/shard_map/gather | solution.py:142
  189.2 1.7 reshape.227
  190.9 2.1 %multiply_reduce_fusion = bf16[256,512]{1,0:T(8,128)(2,1)} fusion(f32[256,2,512]{2,1,0:T(2,128)S(1)} %reshape.227, f32[256,2]{1,0:T(8,128)S(1)} %copy.88), kind=kLoop, calls=%fused_computation.31 | loop fusion | flops 393216 | bytes 1312768 | tf_op jit(solution)/shard_map/reduce_sum | solution.py:143
  (110 shorter events, 34.2 us)
Async XLA Ops:
  7.2 176.8 %copy-start = (bf16[2048,512]{1,0:T(8,128)(2,1)S(1)}, bf16[2048,512]{1,0:T(8,128)(2,1)}, u32[]{:S(2)}) copy-start(bf16[2048,512]{1,0:T(8,128)(2,1)} %param.22) | copy-start | bytes 6291460
  20.5 6.6 %copy-start.8 = (bf16[256,512]{1,0:T(8,128)(2,1)S(1)}, bf16[256,512]{1,0:T(8,128)(2,1)}, u32[]{:S(2)}) copy-start(bf16[256,512]{1,0:T(8,128)(2,1)} %param.17) | copy-start | bytes 786436
  20.5 72.5 %all-to-all-start = ((bf16[8,64,2048]{2,1,0:T(8,128)(2,1)}), bf16[8,64,2048]{2,1,0:T(8,128)(2,1)}, u32[]{:S(2)}, u32[]{:S(2)}) async-start(bf16[8,64,2048]{2,1,0:T(8,128)(2,1)} %bitcast.100), calls=%async_computation | async-start | bytes 4194304 | tf_op jit(solution)/shard_map/all_to_all | solution.py:131
  26.9 94.2 %all-gather.10.cloned.1.call-start = ((), (), s32[]{:S(2)}) async-start(), calls=%async_computation.4 | async-start | bytes 2359296 | tf_op jit(solution)/shard_map/all_gather | solution.py:11
  28.6 5.2 %copy-start.9 = (f32[256,4]{0,1:T(4,128)S(1)}, f32[256,4]{0,1:T(4,128)}, u32[]{:S(2)}) copy-start(f32[256,4]{0,1:T(4,128)} %param.21) | copy-start | bytes 12292
  39.4 0.7 copy-start.2
  43.5 0.7 copy-start.1
  44.2 110.9 %all-gather.8.cloned.1.call-start = ((), (), s32[]{:S(2)}) async-start(), calls=%async_computation.3 | async-start | bytes 5242880 | tf_op jit(solution)/shard_map/all_gather | solution.py:137
  92.9 5.3 %copy-start.11 = (bf16[1,2048,1024]{2,1,0:T(8,128)(2,1)S(1)}, bf16[1,2048,1024]{2,1,0:T(8,128)(2,1)}, u32[]{:S(2)}) copy-start(bf16[1,2048,1024]{2,1,0:T(8,128)(2,1)} %param.28) | copy-start | bytes 12582916
  98.2 5.4 %copy-start.12 = (u32[32]{0:T(128)S(1)}, u32[32]{0:T(128)}, u32[]{:S(2)}) copy-start(u32[32]{0:T(128)} %constant.105) | copy-start | bytes 388
  98.3 22.2 %copy-start.7 = (bf16[256,4,64]{0,2,1:T(8,128)(2,1)S(1)}, bf16[256,4,64]{0,2,1:T(8,128)(2,1)}, u32[]{:S(2)}) copy-start(bf16[256,4,64]{0,2,1:T(8,128)(2,1)} %get-tuple-element.183) | copy-start | bytes 393220
  98.3 22.4 %copy-start.6 = (bf16[256,4,64]{0,2,1:T(8,128)(2,1)S(1)}, bf16[256,4,64]{0,2,1:T(8,128)(2,1)}, u32[]{:S(2)}) copy-start(bf16[256,4,64]{0,2,1:T(8,128)(2,1)} %get-tuple-element.184) | copy-start | bytes 393220
  103.5 17.5 %copy-start.5 = (f32[2,128,4]{2,1,0:T(8,128)S(1)}, f32[2,128,4]{2,1,0:T(8,128)}, u32[]{:S(2)}) copy-start(f32[2,128,4]{2,1,0:T(8,128)} %get-tuple-element.191) | copy-start | bytes 12292
  103.5 80.5 %all-gather.6.cloned.1.call-start = ((), (), s32[]{:S(2)}) async-start(), calls=%async_computation.2 | async-start | bytes 1310720 | tf_op jit(solution)/shard_map/all_gather | solution.py:101
  121.2 14.9 %copy-start.3 = (bf16[2,128,4,128]{3,1,2,0:T(8,128)(2,1)S(1)}, bf16[2,128,4,128]{3,1,2,0:T(8,128)(2,1)}, u32[]{:S(2)}) copy-start(bf16[2,128,4,128]{3,1,2,0:T(8,128)(2,1)} %copy-done.2) | copy-start | bytes 786436
  121.2 14.9 %copy-start.4 = (bf16[2,128,4,128]{3,2,1,0:T(4,128)(2,1)S(1)}, bf16[2,128,4,128]{3,2,1,0:T(4,128)(2,1)}, u32[]{:S(2)}) copy-start(bf16[2,128,4,128]{3,2,1,0:T(4,128)(2,1)} %reshape.218) | copy-start | bytes 786436
  142.2 24.2 %copy-start.10 = (f32[256,2]{0,1:T(2,128)S(1)}, f32[256,2]{0,1:T(2,128)}, u32[]{:S(2)}) copy-start(f32[256,2]{0,1:T(2,128)} %param.26) | copy-start | bytes 6148
  161.8 24.8 %all-to-all-start.1 = ((bf16[8,64,512]{2,1,0:T(8,128)(2,1)}), bf16[8,64,512]{2,1,0:T(8,128)(2,1)S(1)}, u32[]{:S(2)}, u32[]{:S(2)}) async-start(bf16[8,64,512]{2,1,0:T(8,128)(2,1)} %fusion.14), calls=%async_computation.1 | async-start | bytes 1048576 | tf_op jit(solution)/shard_map/all_to_all | solution.py:141
Sparse Core Ops, SparseCore 0:
  44.3 48.1 all-gather.9
  103.6 51.5 all-gather.7
  157.6 26.3 all-gather.5
where the time goes:
time: 201 us; the launch traced here: 200 us
  waiting for transfers between devices  79.1 us (39%)
  local copies, waits for them, and re-layouts  30.9 us (15%)
  matrix products  26.4 us (13%)
  other arithmetic  22.1 us (11%)
  between operations  14.8 us (7%)
  blocking collectives  14.7 us (7%)
  starting transfers between devices  11.2 us (6%)
    all_to_all x1, waiting for transfers between devices, expert_half(): lax.all_to_all(outgoing, 'ep', split_axis=0, concat_axis=0, tiled=True)  48.7 us
    all_gather x1, waiting for transfers between devices, retention_half(): lax.all_gather(head_out, 'tp', axis=1, tiled=True)  17.4 us
    unnamed x1, blocking collectives  14.7 us
    all_gather x1, waiting for transfers between devices, expert_half(): lax.all_gather(hidden, 'tp', axis=2, tiled=True)  13 us
    select_n x7, other arithmetic, turn(): jnp.where(position < mine, new, old)  7.41 us
    dot_general x1, matrix products, expert_half(): jnp.einsum('scf,fd->scd', lax.all_gather(hidden, 'tp', axis=2, tiled=True...  6.6 us
    all_to_all x1, starting transfers between devices, expert_half(): lax.all_to_all(outgoing, 'ep', split_axis=0, concat_axis=0, tiled=True)  6.49 us
    dot_general x1, matrix products, expert_half(): jnp.einsum('scd,df->scf', arrived_rows, w_gate, preferred_element_type=jn...  5.3 us
  transfers between devices with their start and end apart: 5, of which 3 were waited for; matrix products, arithmetic and copies ran while one was open for 29% of the time, Pallas kernels for 0%

commit v1 on v0

--- a/solution.py
+++ b/solution.py
@@ -4,6 +4,19 @@
 from jax.sharding import PartitionSpec as P
 
 BLOCK = 128
+
+
+def gather_around(value, axis, dim):
+    ways = lax.axis_size(axis)
+    up = [(d, (d + 1) % ways) for d in range(ways)]
+    down = [(d, (d - 1) % ways) for d in range(ways)]
+    earlier, later = ([value], [value])
+    for _ in range(ways // 2):
+        earlier.append(lax.ppermute(earlier[-1], axis, up))
+    for _ in range((ways - 1) // 2):
+        later.append(lax.ppermute(later[-1], axis, down))
+    line = jnp.concatenate([*earlier[::-1], *later[1:]], axis=dim)
+    return jnp.roll(line, (lax.axis_index(axis) - ways // 2) * value.shape[dim], axis=dim)
 
 
 def carried_in(value, axis, join, neutral):
@@ -133,10 +146,7 @@
     up_part = jnp.einsum("scd,df->scf", arrived_rows, w_up, preferred_element_type=jnp.float32)
     hidden = (jax.nn.silu(gate_part) * up_part).astype(jnp.bfloat16)
     expert_out = jnp.einsum(
-        "scf,fd->scd",
-        lax.all_gather(hidden, "tp", axis=2, tiled=True),
-        w_down,
-        preferred_element_type=jnp.float32,
+        "scf,fd->scd", gather_around(hidden, "tp", 2), w_down, preferred_element_type=jnp.float32
     ).astype(jnp.bfloat16)
     returned = lax.all_to_all(expert_out, "ep", split_axis=0, concat_axis=0, tiled=True)
     picked = returned.reshape(experts * capacity, -1)[target].reshape(row_count, 2, -1)

time: 201 us -> 233 us (1.16)
  local copies, waits for them, and re-layouts: 30.9 us -> 48.9 us
  waiting for transfers between devices: 79.1 us -> 92.8 us
  matrix products: 26.4 us -> 22.4 us
  starting transfers between devices: 11.2 us -> 13.6 us
    ppermute x0 -> x3, waiting for transfers between devices: none -> 31.8 us  [the longest x2 31.8 us: gather_around(): earlier.append(lax.ppermute(earlier[-1], axis, up))]
    all_gather x1, waiting for transfers between devices: 17.4 us -> 0.02 us  [retention_half(): lax.all_gather(head_out, 'tp', axis=1, tiled=True)]
    all_gather x1 -> x0, waiting for transfers between devices: 13 us -> none  [expert_half(): lax.all_gather(hidden, 'tp', axis=2, tiled=True)]
    all_to_all x1, waiting for transfers between devices: 0.01 us -> 12.4 us  [expert_half(): lax.all_to_all(expert_out, 'ep', split_axis=0, concat_axis=0, tiled=True)]
    unnamed x31 -> x32, local copies, waits for them, and re-layouts: 3.29 us -> 12 us
    concatenate x8, local copies, waits for them, and re-layouts: 4.67 us -> 10.9 us  [rotate(): jnp.concatenate([first_half * cosine - second_half * sine_part, first_hal...]
    ppermute x0 -> x3, starting transfers between devices: none -> 3.57 us  [the longest x2 2.13 us: gather_around(): earlier.append(lax.ppermute(earlier[-1], axis, up))]
    dot_general x1, matrix products: 6.6 us -> 3.15 us  [expert_half(): jnp.einsum('scf,fd->scd', gather_around(hidden, 'tp', 2), w_down, preferr...]
  transfers between devices with their start and end apart: 5 -> 7, of which waited for: 3 -> 3; matrix products, arithmetic and copies ran while one was open for 29% -> 32% of each run, Pallas kernels for 0% -> 0%
where the time goes in v1:
time: 233 us; the launch traced here: 231 us
  waiting for transfers between devices  92.8 us (40%)
  local copies, waits for them, and re-layouts  48.9 us (21%)
  other arithmetic  24 us (10%)
  matrix products  22.4 us (10%)
  between operations  15 us (6%)
  blocking collectives  14.4 us (6%)
  starting transfers between devices  13.6 us (6%)
    all_to_all x1, waiting for transfers between devices, expert_half(): lax.all_to_all(outgoing, 'ep', split_axis=0, concat_axis=0, tiled=True)  48.6 us
    ppermute x2, waiting for transfers between devices, gather_around(): earlier.append(lax.ppermute(earlier[-1], axis, up))  31.8 us
    unnamed x1, blocking collectives  14.4 us
    all_to_all x1, waiting for transfers between devices, expert_half(): lax.all_to_all(expert_out, 'ep', split_axis=0, concat_axis=0, tiled=True)  12.4 us
    unnamed x32, local copies, waits for them, and re-layouts  12 us
    concatenate x8, local copies, waits for them, and re-layouts, rotate(): jnp.concatenate([first_half * cosine - second_half * sine_part, first_hal...  10.9 us
    select_n x7, other arithmetic, turn(): jnp.where(position < mine, new, old)  7.34 us
    all_to_all x1, starting transfers between devices, expert_half(): lax.all_to_all(outgoing, 'ep', split_axis=0, concat_axis=0, tiled=True)  6.49 us
  transfers between devices with their start and end apart: 7, of which 3 were waited for; matrix products, arithmetic and copies ran while one was open for 32% of the time, Pallas kernels for 0%

profile of v1, /device:TPU:0, one launch (start us, length us, event | category | flops | bytes accessed | tf_op | source)
XLA Modules:
  0.0 231.3 jit_solution(5410723015288783803)
XLA Ops:
  10.9 2.4 %scatter_custom_fusion = s32[512]{0:T(512)S(1)} fusion(s32[512]{0:T(512)S(1)} %bitcast.109, s32[512]{0:T(512)S(1)} %add_select_fusion, s32[]{:T(128)} %copy.132), kind=kCustom, calls=%fused_computation.99 | custom fusion | bytes 2052 | tf_op jit(solution)/shard_map/scatter | solution.py:138
  17.2 3.3 %gather_fusion = bf16[512,2048]{1,0:T(8,128)(2,1)} fusion(bf16[256,2048]{1,0:T(8,128)(2,1)S(1)} %fusion.12, s32[1024]{0:T(1024)S(1)} %pad_clamp_fusion.1), kind=kCustom, calls=%fused_computation | custom fusion | bytes 4196352 | tf_op jit(solution)/shard_map/gather | solution.py:140
  20.5 6.5 %all-to-all-start = ((bf16[8,64,2048]{2,1,0:T(8,128)(2,1)}), bf16[8,64,2048]{2,1,0:T(8,128)(2,1)}, u32[]{:S(2)}, u32[]{:S(2)}) async-start(bf16[8,64,2048]{2,1,0:T(8,128)(2,1)} %bitcast.99), calls=%async_computation | async-start | bytes 4194304 | tf_op jit(solution)/shard_map/all_to_all | solution.py:144
  30.9 1.8 concatenate.27
  37.5 1.7 reshape.218
  41.9 1.7 while.29
  44.3 48.6 %all-to-all-done = bf16[8,64,2048]{2,1,0:T(8,128)(2,1)} async-done(((bf16[8,64,2048]{2,1,0:T(8,128)(2,1)}), bf16[8,64,2048]{2,1,0:T(8,128)(2,1)}, u32[]{:S(2)}, u32[]{:S(2)}) %all-to-all-start) | async-done | bytes 2097184 | tf_op jit(solution)/shard_map/all_to_all | solution.py:144
  93.0 5.3 %fusion.7 = f32[8,64,1024]{2,1,0:T(8,128)S(1)} fusion(bf16[8,64,2048]{2,1,0:T(8,128)(2,1)} %all-to-all-done, bf16[1,2048,1024]{2,1,0:T(8,128)(2,1)} %param.27), kind=kOutput, calls=%fused_computation.15 | convolution fusion | flops 2147483648 | bytes 8388608 | tf_op jit(solution)/shard_map/scd,df->scf/dot_general | solution.py:145
  98.3 4.1 %multiply_convert_fusion = bf16[8,64,1024]{2,1,0:T(8,128)(2,1)S(1)} fusion(f32[8,64,1024]{2,1,0:T(8,128)S(1)} %fusion.7, bf16[8,64,2048]{2,1,0:T(8,128)(2,1)} %all-to-all-done, bf16[1,2048,1024]{2,1,0:T(8,128)(2,1)S(1)} %copy-done.7), kind=kOutput, calls=%fused_computation.23 | convolution fusion | flops 2150629376 | bytes 9437184 | tf_op jit(solution)/shard_map/scd,df->scf/dot_general | solution.py:146
  107.7 14.4 %all-reduce = f32[32]{0:T(128)S(1)} all-reduce(f32[32]{0:T(128)} %exponential_dynamic-update-slice_fusion), channel_id=2, replica_groups=mesh['ep'=8,'tp'=4] {'ep'}, use_global_device_ids=true, to_apply=%add | all-reduce | flops 32 | bytes 256
  124.3 1.8 copy.68
  127.7 1.8 copy.69
  133.8 12.2 %while.30 = (s32[]{:T(128)}, f32[4,128,128]{2,1,0:T(8,128)S(1)}, s32[]{:T(128)}, f32[8,4]{1,0:T(8,128)}, f32[8,4,128,128]{3,2,1,0:T(8,128)}) while((s32[]{:T(128)}, f32[4,128,128]{2,1,0:T(8,128)S(1)}, s32[]{:T(128)}, f32[8,4]{1,0:T(8,128)}, f32[8,4,128,128]{3,2,1,0:T(8,128)}) %tuple.77), condition=%wide.region_6.7_spmd.clone.clone, body=%wide.region_5.6_spmd.clone.sunk.clone | while | flops 262148 | bytes 786569 | solution.py:33
  146.1 2.7 %fusion.21 = f32[2,128,4,128]{1,3,2,0:T(8,128)} fusion(f32[2,4,128,128]{3,2,1,0:T(8,128)} %get-tuple-element.124, f32[2,128,4]{1,2,0:T(4,128)S(1)} %copy.82, f32[4,128,128]{2,1,0:T(8,128)S(1)} %get-tuple-element.126, f32[2,4]{1,0:T(2,128)S(1)} %subtract_exponential_fusion.1, bf16[2,128,4,64]{3,1,2,0:T(8,128)(2,1)} %copy.69, bf16[2,128,4,64]{3,1,2,0:T(8,128)(2,1)} %copy.68), kind=kOutput, calls=%fused_computation.29 | convolution fusion | flops 202244096 | bytes 1576992 | tf_op jit(solution)/shard_map/nihd,nhde->nihe/dot_general | solution.py:101
  148.8 2.8 %multiply_reduce_fusion.1 = (f32[2,128,4]{1,2,0:T(4,128)S(1)}, f32[2,128,4,128]{1,3,2,0:T(8,128)}) fusion(f32[2,128,4,128]{1,3,2,0:T(8,128)} %fusion.21, bf16[2,128,4,128]{3,2,1,0:T(4,128)(2,1)} %reshape.218, bf16[2,128,4,128]{3,1,2,0:T(8,128)(2,1)} %copy-done.2, f32[2,4,128]{2,1,0:T(4,128)S(1)} %copy.75, pred[128,128]{1,0:T(8,128)(4,1)} %iota_compare_fusion, ...), kind=kOutput, calls=%fused_computation.42 | convolution fusion | flops 68680704 | bytes 1859584 | tf_op jit(solution)/shard_map/nhij,njhd->nihd/dot_general | solution.py:82
  151.7 2.0 copy.83
  154.1 1.9 fusion.37
  156.1 31.8 %collective-permute-done.1 = bf16[8,64,1024]{2,1,0:T(8,128)(2,1)} collective-permute-done((bf16[8,64,1024]{2,1,0:T(8,128)(2,1)}, bf16[8,64,1024]{2,1,0:T(8,128)(2,1)}, u32[]{:S(2)}, u32[]{:S(2)}) %collective-permute-start.1) | collective-permute-done | bytes 1048608 | tf_op jit(solution)/shard_map/ppermute | solution.py:15
  196.2 3.1 %fusion.15 = bf16[8,64,512]{2,1,0:T(8,128)(2,1)} fusion(bf16[1,4096,512]{2,1,0:T(8,128)(2,1)S(1)} %copy-done.8, bf16[8,64,8192]{2,1,0:T(8,128)(2,1)S(1)} %constant_dynamic-update-slice_fusion, s32[]{:T(128)S(6)} %select_n.67), kind=kOutput, calls=%fused_computation.24 | convolution fusion | flops 2147745792 | bytes 8912900 | tf_op jit(solution)/shard_map/scf,fd->scd/dot_general | solution.py:148
  199.4 3.5 %all-to-all-start.1 = ((bf16[8,64,512]{2,1,0:T(8,128)(2,1)}), bf16[8,64,512]{2,1,0:T(8,128)(2,1)S(1)}, u32[]{:S(2)}, u32[]{:S(2)}) async-start(bf16[8,64,512]{2,1,0:T(8,128)(2,1)} %fusion.15), calls=%async_computation.1 | async-start | bytes 1048576 | tf_op jit(solution)/shard_map/all_to_all | solution.py:151
  203.1 2.6 %convolution_convert_fusion = bf16[256,512]{1,0:T(8,128)(2,1)} fusion(bf16[256,2048]{1,0:T(8,128)(2,1)} %all-gather.5.cloned.1.call-done, bf16[2048,512]{1,0:T(8,128)(2,1)S(1)} %copy-done), kind=kOutput, calls=%fused_computation.30 | convolution fusion | flops 537001984 | bytes 3407872 | tf_op jit(solution)/shard_map/dot_general | solution.py:113
  205.7 12.4 %all-to-all-done.1 = bf16[8,64,512]{2,1,0:T(8,128)(2,1)S(1)} async-done(((bf16[8,64,512]{2,1,0:T(8,128)(2,1)}), bf16[8,64,512]{2,1,0:T(8,128)(2,1)S(1)}, u32[]{:S(2)}, u32[]{:S(2)}) %all-to-all-start.1) | async-done | bytes 524320 | tf_op jit(solution)/shard_map/all_to_all | solution.py:151
  218.1 2.6 %gather_fusion.1 = bf16[512,512]{1,0:T(8,128)(2,1)} fusion(bf16[512,512]{1,0:T(8,128)(2,1)S(1)} %bitcast.98, s32[1024]{0:T(1024)S(1)} %pad_clamp_fusion), kind=kCustom, calls=%fused_computation.1 | custom fusion | bytes 1050624 | tf_op jit(solution)/shard_map/gather | solution.py:152
  222.4 2.1 multiply_reduce_fusion
  (115 shorter events, 56.8 us)
Async XLA Ops:
  7.2 195.9 %copy-start = (bf16[2048,512]{1,0:T(8,128)(2,1)S(1)}, bf16[2048,512]{1,0:T(8,128)(2,1)}, u32[]{:S(2)}) copy-start(bf16[2048,512]{1,0:T(8,128)(2,1)} %param.22) | copy-start | bytes 6291460
  20.5 6.6 %copy-start.3 = (bf16[256,512]{1,0:T(8,128)(2,1)S(1)}, bf16[256,512]{1,0:T(8,128)(2,1)}, u32[]{:S(2)}) copy-start(bf16[256,512]{1,0:T(8,128)(2,1)} %param.17) | copy-start | bytes 786436
  20.5 72.5 %all-to-all-start = ((bf16[8,64,2048]{2,1,0:T(8,128)(2,1)}), bf16[8,64,2048]{2,1,0:T(8,128)(2,1)}, u32[]{:S(2)}, u32[]{:S(2)}) async-start(bf16[8,64,2048]{2,1,0:T(8,128)(2,1)} %bitcast.99), calls=%async_computation | async-start | bytes 4194304 | tf_op jit(solution)/shard_map/all_to_all | solution.py:144
  27.0 6.9 %copy-start.5 = (f32[256,4]{0,1:T(4,128)S(1)}, f32[256,4]{0,1:T(4,128)}, u32[]{:S(2)}) copy-start(f32[256,4]{0,1:T(4,128)} %param.21) | copy-start | bytes 12292
  27.0 106.9 %all-gather.7.cloned.1.call-start = ((), (), s32[]{:S(2)}) async-start(), calls=%async_computation.3 | async-start | bytes 2359296 | tf_op jit(solution)/shard_map/all_gather | solution.py:24
  39.4 0.7 copy-start.2
  43.6 0.7 copy-start.1
  44.3 158.8 %all-gather.5.cloned.1.call-start = ((), (), s32[]{:S(2)}) async-start(), calls=%async_computation.2 | async-start | bytes 1310720 | tf_op jit(solution)/shard_map/all_gather | solution.py:114
  93.0 5.3 %copy-start.7 = (bf16[1,2048,1024]{2,1,0:T(8,128)(2,1)S(1)}, bf16[1,2048,1024]{2,1,0:T(8,128)(2,1)}, u32[]{:S(2)}) copy-start(bf16[1,2048,1024]{2,1,0:T(8,128)(2,1)} %param.28) | copy-start | bytes 12582916
  98.3 6.3 %copy-start.9 = (u32[32]{0:T(128)S(1)}, u32[32]{0:T(128)}, u32[]{:S(2)}) copy-start(u32[32]{0:T(128)} %constant.133) | copy-start | bytes 388
  102.4 30.8 %collective-permute-start = (bf16[8,64,1024]{2,1,0:T(8,128)(2,1)S(1)}, bf16[8,64,1024]{2,1,0:T(8,128)(2,1)}, u32[]{:S(2)}, u32[]{:S(2)}) collective-permute-start(bf16[8,64,1024]{2,1,0:T(8,128)(2,1)S(1)} %multiply_convert_fusion), channel_id=1, source_target_pairs={{0,1},{1,2},{2,3},{3,0},{4,5},{5,6},{6,7},{7,4},{8,9},{9,10},{10,1... | collective-permute-start | bytes 3145736 | tf_op jit(solution)/shard_map/ppermute | solution.py:15
  131.8 58.8 %collective-permute-start.2 = (bf16[8,64,1024]{2,1,0:T(8,128)(2,1)S(1)}, bf16[8,64,1024]{2,1,0:T(8,128)(2,1)}, u32[]{:S(2)}, u32[]{:S(2)}) collective-permute-start(bf16[8,64,1024]{2,1,0:T(8,128)(2,1)S(1)} %multiply_convert_fusion), channel_id=1, source_target_pairs={{0,3},{1,0},{2,1},{3,2},{4,7},{5,4},{6,5},{7,6},{8,11},{9,8},{10,9... | collective-permute-start | bytes 3145736 | tf_op jit(solution)/shard_map/ppermute | solution.py:17
  133.2 54.6 %collective-permute-start.1 = (bf16[8,64,1024]{2,1,0:T(8,128)(2,1)}, bf16[8,64,1024]{2,1,0:T(8,128)(2,1)}, u32[]{:S(2)}, u32[]{:S(2)}) collective-permute-start(bf16[8,64,1024]{2,1,0:T(8,128)(2,1)} %collective-permute-done), channel_id=1, source_target_pairs={{0,1},{1,2},{2,3},{3,0},{4,5},{5,6},{6,7},{7,4},{8,9},{9,10},{10,1... | collective-permute-start | bytes 3145736 | tf_op jit(solution)/shard_map/ppermute | solution.py:15
  148.8 5.3 %copy-start.4 = (bf16[256,512]{1,0:T(8,128)(2,1)S(1)}, bf16[256,512]{1,0:T(8,128)(2,1)}, u32[]{:S(2)}) copy-start(bf16[256,512]{1,0:T(8,128)(2,1)} %param.20) | copy-start | bytes 786436
  191.9 4.3 %copy-start.8 = (bf16[1,4096,512]{2,1,0:T(8,128)(2,1)S(1)}, bf16[1,4096,512]{2,1,0:T(8,128)(2,1)}, u32[]{:S(2)}) copy-start(bf16[1,4096,512]{2,1,0:T(8,128)(2,1)} %param.29) | copy-start | bytes 12582916
  196.2 6.7 %copy-start.6 = (f32[256,2]{0,1:T(2,128)S(1)}, f32[256,2]{0,1:T(2,128)}, u32[]{:S(2)}) copy-start(f32[256,2]{0,1:T(2,128)} %param.26) | copy-start | bytes 6148
  199.4 18.8 %all-to-all-start.1 = ((bf16[8,64,512]{2,1,0:T(8,128)(2,1)}), bf16[8,64,512]{2,1,0:T(8,128)(2,1)S(1)}, u32[]{:S(2)}, u32[]{:S(2)}) async-start(bf16[8,64,512]{2,1,0:T(8,128)(2,1)} %fusion.15), calls=%async_computation.1 | async-start | bytes 1048576 | tf_op jit(solution)/shard_map/all_to_all | solution.py:151
Sparse Core Ops, SparseCore 0:
  44.4 48.1 all-gather.6
  156.2 31.9 all-gather.4
